TPU v7x, 32 devices: a whole 2x2x4 slice. The times are simulated.
32 devices in a mesh: fs: 16 (over z, y, x), tp: 2 (over core).
Axes of the slice: x: 2, y: 2, z: 4, core: 2. Of those that a mesh axis runs over, the one named last changes fastest.
Arguments:
- tokens: bfloat16 [8192, 2048], P('fs', 'tp'), may hold values from -6 to 6
- norm_gain: bfloat16 [2048], P('tp'), may hold values from 0.099609375 to 1.8984375
- proj_u: bfloat16 [2048, 2048], P('fs', 'tp'), may hold values from -0.125 to 0.125
- proj_v: bfloat16 [2048, 2048], P('fs', 'tp'), may hold values from -0.125 to 0.125
- layer_gain: bfloat16 [2048], P('tp'), may hold values from 0.099609375 to 1.8984375
- layer_shift: bfloat16 [2048], P('tp'), may hold values from -3 to 3
- mix_weight: bfloat16 [16, 128, 128], P('tp'), may hold values from -0.5 to 0.5
- mix_bias: bfloat16 [16, 128], P('tp'), may hold values from 0.099609375 to 1.8984375
- proj_out: bfloat16 [2048, 2048], P('tp', 'fs'), may hold values from -0.1875 to 0.1875
- ffn_gain: bfloat16 [2048], P('tp'), may hold values from 0.099609375 to 1.8984375
- ffn_gate: bfloat16 [2048, 4096], P('fs', 'tp'), may hold values from -0.125 to 0.125
- ffn_value: bfloat16 [2048, 4096], P('fs', 'tp'), may hold values from -0.125 to 0.125
- conv_gate: bfloat16 [3, 4096], P(None, 'tp'), may hold values from -3 to 3
- conv_value: bfloat16 [3, 4096], P(None, 'tp'), may hold values from -3 to 3
- proj_down: bfloat16 [4096, 2048], P('tp', 'fs'), may hold values from -0.125 to 0.125
Outputs:
- result: bfloat16 [8192, 2048], P('fs', 'tp')
All inputs are finite; a program needn't handle non-finite values.
Results may differ from a plain program's by a relative error of at most 0.017.
Values may be sent and summed in bfloat16 or wider, within the bound.
A program may use at most 64 MiB of HBM per device.

v0:
```python
import jax
import jax.numpy as jnp
from jax import lax
from jax.sharding import PartitionSpec as P

GROUP_DIM = 128
BLOCK = 128
SEGMENT = 64
KERNEL = 3
SEQ_LEN = 256
EPS = 1e-06


def matmul(operand, matrix):
    return jnp.dot(operand, matrix, preferred_element_type=jnp.float32)


def local_rms(values_in, gain_row):
    values = values_in.astype(jnp.float32)
    scale_row = lax.rsqrt(jnp.mean(values * values, axis=1, keepdims=True) + EPS)
    return (values * scale_row * gain_row.astype(jnp.float32)).astype(jnp.bfloat16)


def causal_taps(values, weights):
    seq_count = values.shape[0] // SEQ_LEN
    shaped = values.reshape(seq_count, SEQ_LEN, values.shape[1])
    padded = jnp.pad(shaped, ((0, 0), (KERNEL - 1, 0), (0, 0)))
    summed = jnp.zeros(shaped.shape, jnp.float32)
    for tap_index in range(KERNEL):
        summed = summed + padded[:, tap_index : tap_index + SEQ_LEN].astype(jnp.float32) * weights[
            tap_index
        ].astype(jnp.float32)
    return summed.reshape(values.shape[0], values.shape[1])


def on_device(
    tokens,
    norm_gain,
    proj_u,
    proj_v,
    layer_gain,
    layer_shift,
    mix_weight,
    mix_bias,
    proj_out,
    ffn_gain,
    ffn_gate,
    ffn_value,
    conv_gate,
    conv_value,
    proj_down,
):
    own_width = tokens.shape[1]
    whole_tokens, whole_gain, whole_ffn_gain = (
        lax.all_gather(tokens, "tp", axis=1, tiled=True),
        lax.all_gather(norm_gain, "tp", axis=0, tiled=True),
        lax.all_gather(ffn_gain, "tp", axis=0, tiled=True),
    )
    normed = local_rms(whole_tokens, whole_gain)
    row_count = normed.shape[0]
    whole_u, whole_v = (
        lax.all_gather(proj_u, "fs", axis=0, tiled=True),
        lax.all_gather(proj_v, "fs", axis=0, tiled=True),
    )
    pre_u = matmul(normed, whole_u)
    pre_v = matmul(normed, whole_v)
    act_u = jax.nn.gelu(pre_u, approximate=False)
    act_v = jax.nn.gelu(pre_v, approximate=False)
    full_width = act_v.shape[1] * lax.axis_size("tp")
    total_sum, second = lax.psum((jnp.sum(act_v, axis=1), jnp.sum(act_v * act_v, axis=1)), "tp")
    center = total_sum / full_width
    spread = second / full_width - center * center
    mixed_in = (
        (act_v - center[:, None])
        * lax.rsqrt(spread + EPS)[:, None]
        * layer_gain.astype(jnp.float32)
        + layer_shift.astype(jnp.float32)
    ).astype(jnp.bfloat16)
    groups = mixed_in.shape[1] // GROUP_DIM
    blocks = mixed_in.reshape(row_count // BLOCK, BLOCK, groups, GROUP_DIM)
    segment = jnp.arange(BLOCK) // SEGMENT
    visible = segment[None, :] <= segment[:, None]
    masked = jnp.where(visible[None], mix_weight, jnp.zeros_like(mix_weight))
    spatial = (
        jnp.einsum("gij,njgc->nigc", masked, blocks, preferred_element_type=jnp.float32)
        + mix_bias.astype(jnp.float32).T[None, :, :, None]
    )
    gated_rows = (act_u * spatial.reshape(row_count, mixed_in.shape[1])).astype(jnp.bfloat16)
    whole_out = lax.all_gather(proj_out, "fs", axis=1, tiled=True)
    partial_value = matmul(gated_rows, whole_out)
    summed = lax.psum(partial_value.astype(jnp.bfloat16), "tp").astype(jnp.float32)
    stream_rows = (whole_tokens.astype(jnp.float32) + summed).astype(jnp.bfloat16)
    normed_two = local_rms(stream_rows, whole_ffn_gain)
    stream = lax.dynamic_slice_in_dim(stream_rows, lax.axis_index("tp") * own_width, own_width, 1)
    whole_gate, whole_value = (
        lax.all_gather(ffn_gate, "fs", axis=0, tiled=True),
        lax.all_gather(ffn_value, "fs", axis=0, tiled=True),
    )
    pre_gate = matmul(normed_two, whole_gate)
    pre_value = matmul(normed_two, whole_value)
    conv_g = causal_taps(pre_gate.astype(jnp.bfloat16), conv_gate)
    conv_v = causal_taps(pre_value.astype(jnp.bfloat16), conv_value)
    hidden = (jax.nn.silu(conv_g) * conv_v).astype(jnp.bfloat16)
    whole_down = lax.all_gather(proj_down, "fs", axis=1, tiled=True)
    partial_two = matmul(hidden, whole_down)
    return (
        stream.astype(jnp.float32)
        + lax.psum_scatter(
            partial_two.astype(jnp.bfloat16), "tp", scatter_dimension=1, tiled=True
        ).astype(jnp.float32)
    ).astype(jnp.bfloat16)


def solution(mesh):
    in_specs = (
        P("fs", "tp"),
        P("tp"),
        P("fs", "tp"),
        P("fs", "tp"),
        P("tp"),
        P("tp"),
        P("tp", None, None),
        P("tp", None),
        P("tp", "fs"),
        P("tp"),
        P("fs", "tp"),
        P("fs", "tp"),
        P(None, "tp"),
        P(None, "tp"),
        P("tp", "fs"),
    )
    out_specs = P("fs", "tp")
    return jax.shard_map(
        on_device, mesh=mesh, in_specs=in_specs, out_specs=out_specs, check_vma=False
    )
```

profile of v0, /device:TPU:0, one launch (start us, length us, event | category | flops | bytes accessed | tf_op | source)
XLA Modules:
  0.0 702.0 jit_solution(10624210363305999877)
XLA Ops:
  6.5 0.0 all-gather.8.cloned.1.call-start
  6.5 0.7 all-gather.8.cloned.1.call-update
  7.3 0.0 all-gather.12.cloned.1.call-start
  7.3 0.7 all-gather.12.cloned.1.call-update
  8.0 0.0 all-gather.10.cloned.1.call-start
  8.1 0.7 all-gather.10.cloned.1.call-update
  8.7 0.0 all-gather.14.cloned.1.call-start
  8.8 0.5 all-gather.14.cloned.1.call-update
  9.3 0.0 all-reduce.5.cloned.1.call-start
  9.4 2.1 all_gather.28
  11.5 0.7 convert_element_type.146
  12.2 0.7 convert_element_type.147
  12.9 0.7 convert_bitcast_fusion
  13.5 0.1 broadcast_compare_fusion
  13.6 8.6 %all-gather.8.cloned.1.call-done = bf16[512,2048]{1,0:T(8,128)(2,1)} async-done(((bf16[512,1024]{1,0:T(8,128)(2,1)}), bf16[512,2048]{1,0:T(8,128)(2,1)}) %all-gather.8.cloned.1.call-update) | async-done | bytes 2097168 | tf_op jit(solution)/shard_map/all_gather | solution.py:55
  22.2 0.0 copy-start
  22.2 2.2 fusion.3
  24.4 77.3 %all-gather.12.cloned.1.call-done = bf16[2048,1024]{1,0:T(8,128)(2,1)} async-done(((bf16[128,1024]{1,0:T(8,128)(2,1)}), bf16[2048,1024]{1,0:T(8,128)(2,1)}) %all-gather.12.cloned.1.call-update) | async-done | bytes 4194320 | tf_op jit(solution)/shard_map/all_gather | solution.py:63
  101.8 0.0 copy-done
  101.8 9.6 %fusion.111 = (f32[512]{0:T(512)S(1)}, f32[512]{0:T(512)S(1)}, f32[512,1024]{1,0:T(8,128)}) fusion(bf16[2048,1024]{1,0:T(8,128)(2,1)} %all-gather.12.cloned.1.call-done, bf16[512,2048]{1,0:T(8,128)(2,1)S(1)} %copy-done, f32[2048]{0:T(1024)S(1)} %convert_element_type.144, f32[512]{0:T(512)S(1)} %add_rsqrt_fusion.2), kind=kOutput, calls=%fused_computation.152 | convolution fusion | flops 2186804224 | bytes 8402944 | tf_op jit(solution)/shard_map/dot_general | solution.py:15
  111.4 2.6 all-reduce.2
  114.1 0.0 copy-start.3
  114.1 2.1 fusion.32
  116.2 0.3 copy.21
  116.4 0.0 copy-done.3
  116.4 1.9 bitcast_add_fusion
  118.3 2.9 copy.19
  121.2 57.5 %all-gather.10.cloned.1.call-done = bf16[2048,1024]{1,0:T(8,128)(2,1)} async-done(((bf16[128,1024]{1,0:T(8,128)(2,1)}), bf16[2048,1024]{1,0:T(8,128)(2,1)}) %all-gather.10.cloned.1.call-update) | async-done | bytes 4194320 | tf_op jit(solution)/shard_map/all_gather | solution.py:62
  178.8 89.9 %all-gather.14.cloned.1.call-done = bf16[1024,2048]{1,0:T(8,128)(2,1)} async-done(((bf16[1024,128]{1,0:T(8,128)(2,1)}), bf16[1024,2048]{1,0:T(8,128)(2,1)}) %all-gather.14.cloned.1.call-update) | async-done | bytes 4194320 | tf_op jit(solution)/shard_map/all_gather | solution.py:89
  268.7 14.5 %convolution_convert_fusion = bf16[512,2048]{1,0:T(8,128)(2,1)} fusion(bf16[1024,2048]{1,0:T(8,128)(2,1)} %all-gather.14.cloned.1.call-done, f32[64,8,8,128]{3,2,1,0:T(8,128)} %bitcast.51, bf16[2048,1024]{1,0:T(8,128)(2,1)} %all-gather.10.cloned.1.call-done, bf16[512,2048]{1,0:T(8,128)(2,1)S(1)} %copy-done, f32[2048]{0:T(1024)S(1)} %convert_element_type.144, ...), kind=kOutput, calls=%fused_computation.23 | convolution fusion | flops 4334813184 | bytes 14690304 | tf_op jit(solution)/shard_map/dot_general | solution.py:15
  283.2 0.0 copy-start.6
  283.2 0.0 copy-start.4
  283.2 0.0 copy-start.5
  283.2 0.0 all-reduce.5.cloned.1.call-update
  283.2 0.0 all-gather.16.cloned.1.call-start
  283.3 0.5 all-gather.16.cloned.1.call-update
  283.8 0.0 all-gather.18.cloned.1.call-start
  283.8 0.7 all-gather.18.cloned.1.call-update
  284.5 0.0 all-gather.20.cloned.1.call-start
  284.6 0.7 all-gather.20.cloned.1.call-update
  285.3 0.0 reduce-scatter.2.cloned.1.call-start
  285.3 0.0 copy-done.6
  285.3 2.1 all_gather.32
  287.4 0.0 copy-done.4
  287.4 0.0 copy-done.5
  287.5 15.4 %all-reduce.5.cloned.1.call-done = bf16[512,2048]{1,0:T(8,128)(2,1)} async-done(((bf16[512,2048]{1,0:T(8,128)(2,1)}), bf16[512,2048]{1,0:T(8,128)(2,1)}) %all-reduce.5.cloned.1.call-update) | async-done | bytes 2097168 | tf_op jit(solution)/shard_map/psum | solution.py:91
  302.8 3.9 fusion
  306.8 112.2 %all-gather.16.cloned.1.call-done = bf16[2048,2048]{1,0:T(8,128)(2,1)} async-done(((bf16[128,2048]{1,0:T(8,128)(2,1)}), bf16[2048,2048]{1,0:T(8,128)(2,1)}) %all-gather.16.cloned.1.call-update) | async-done | bytes 8388624 | tf_op jit(solution)/shard_map/all_gather | solution.py:96
  419.0 0.0 copy-start.1
  419.0 10.0 %convolution_convert_fusion.3 = bf16[512,2048]{1,0:T(8,128)(2,1)} fusion(bf16[2048,2048]{1,0:T(8,128)(2,1)} %all-gather.16.cloned.1.call-done, bf16[512,2048]{1,0:T(8,128)(2,1)} %get-tuple-element.10, f32[2048]{0:T(1024)S(1)} %convert_element_type.155, f32[512]{0:T(512)S(1)} %add_rsqrt_fusion), kind=kOutput, calls=%fused_computation.26 | convolution fusion | flops 4300210176 | bytes 12593152 | tf_op jit(solution)/shard_map/dot_general | solution.py:15
  429.0 103.2 %all-gather.18.cloned.1.call-done = bf16[2048,2048]{1,0:T(8,128)(2,1)} async-done(((bf16[128,2048]{1,0:T(8,128)(2,1)}), bf16[2048,2048]{1,0:T(8,128)(2,1)}) %all-gather.18.cloned.1.call-update) | async-done | bytes 8388624 | tf_op jit(solution)/shard_map/all_gather | solution.py:97
  532.2 0.0 copy-done.1
  532.2 0.0 copy-start.2
  532.2 8.4 %convolution_convert_fusion.2 = bf16[512,2048]{1,0:T(8,128)(2,1)S(1)} fusion(bf16[2048,2048]{1,0:T(8,128)(2,1)} %all-gather.18.cloned.1.call-done, bf16[512,2048]{1,0:T(8,128)(2,1)S(1)} %copy-done.1, f32[2048]{0:T(1024)S(1)} %convert_element_type.155, f32[512]{0:T(512)S(1)} %add_rsqrt_fusion), kind=kOutput, calls=%fused_computation.25 | convolution fusion | flops 4300210176 | bytes 12593152 | tf_op jit(solution)/shard_map/dot_general | solution.py:15
  540.6 0.0 copy-done.2
  540.7 3.0 multiply_add_fusion
  543.7 2.6 fusion.7
  546.3 128.7 %all-gather.20.cloned.1.call-done = bf16[2048,2048]{1,0:T(8,128)(2,1)} async-done(((bf16[2048,128]{1,0:T(8,128)(2,1)}), bf16[2048,2048]{1,0:T(8,128)(2,1)}) %all-gather.20.cloned.1.call-update) | async-done | bytes 8388624 | tf_op jit(solution)/shard_map/all_gather | solution.py:104
  675.0 9.9 %convolution_convert_fusion.1 = bf16[512,2048]{1,0:T(8,128)(2,1)} fusion(bf16[512,2048]{1,0:T(8,128)(2,1)} %fusion.7, bf16[2048,2048]{1,0:T(8,128)(2,1)} %all-gather.20.cloned.1.call-done), kind=kOutput, calls=%fused_computation.24 | convolution fusion | flops 4296015872 | bytes 12582912 | tf_op jit(solution)/shard_map/dot_general | solution.py:15
  684.9 0.0 reduce-scatter.2.cloned.1.call-update
  684.9 8.0 %reduce-scatter.2.cloned.1.call-done = bf16[512,1024]{1,0:T(8,128)(2,1)} async-done(((bf16[512,2048]{1,0:T(8,128)(2,1)}), bf16[512,1024]{1,0:T(8,128)(2,1)}) %reduce-scatter.2.cloned.1.call-update) | async-done | bytes 1048592 | tf_op jit(solution)/shard_map/reduce_scatter | solution.py:108
  692.9 2.6 add_convert_fusion
  (8 shorter events, 0.1 us)
Async XLA Ops:
  6.5 15.7 %all-gather.8.cloned.1.call-start = ((), (), s32[]{:S(2)}) async-start(), calls=%async_computation.1 | async-start | bytes 3145728 | tf_op jit(solution)/shard_map/all_gather | solution.py:55
  7.3 94.5 %all-gather.12.cloned.1.call-start = ((), (), s32[]{:S(2)}) async-start(), calls=%async_computation.3 | async-start | bytes 4456448 | tf_op jit(solution)/shard_map/all_gather | solution.py:63
  8.0 170.8 %all-gather.10.cloned.1.call-start = ((), (), s32[]{:S(2)}) async-start(), calls=%async_computation.2 | async-start | bytes 4456448 | tf_op jit(solution)/shard_map/all_gather | solution.py:62
  8.7 259.9 %all-gather.14.cloned.1.call-start = ((), (), s32[]{:S(2)}) async-start(), calls=%async_computation.4 | async-start | bytes 4456448 | tf_op jit(solution)/shard_map/all_gather | solution.py:89
  9.3 293.5 %all-reduce.5.cloned.1.call-start = ((), (), s32[]{:S(2)}) async-start(), calls=%async_computation.5 | async-start | bytes 4194304 | tf_op jit(solution)/shard_map/psum | solution.py:91
  22.2 79.6 %copy-start = (bf16[512,2048]{1,0:T(8,128)(2,1)S(1)}, bf16[512,2048]{1,0:T(8,128)(2,1)}, u32[]{:S(2)}) copy-start(bf16[512,2048]{1,0:T(8,128)(2,1)} %all-gather.8.cloned.1.call-done) | copy-start | bytes 6291460
  114.1 2.4 copy-start.3
  283.2 2.2 copy-start.6
  283.2 4.2 copy-start.4
  283.2 4.3 copy-start.5
  283.2 135.8 %all-gather.16.cloned.1.call-start = ((), (), s32[]{:S(2)}) async-start(), calls=%async_computation.6 | async-start | bytes 8912896 | tf_op jit(solution)/shard_map/all_gather | solution.py:96
  283.8 248.4 %all-gather.18.cloned.1.call-start = ((), (), s32[]{:S(2)}) async-start(), calls=%async_computation.7 | async-start | bytes 8912896 | tf_op jit(solution)/shard_map/all_gather | solution.py:97
  284.5 390.4 %all-gather.20.cloned.1.call-start = ((), (), s32[]{:S(2)}) async-start(), calls=%async_computation.8 | async-start | bytes 8912896 | tf_op jit(solution)/shard_map/all_gather | solution.py:104
  285.3 407.6 %reduce-scatter.2.cloned.1.call-start = ((), (), s32[]{:S(2)}) async-start(), calls=%async_computation.9 | async-start | bytes 3145728 | tf_op jit(solution)/shard_map/reduce_scatter | solution.py:108
  419.0 113.3 %copy-start.1 = (bf16[512,2048]{1,0:T(8,128)(2,1)S(1)}, bf16[512,2048]{1,0:T(8,128)(2,1)}, u32[]{:S(2)}) copy-start(bf16[512,2048]{1,0:T(8,128)(2,1)} %get-tuple-element.10) | copy-start | bytes 6291460
  532.2 8.4 %copy-start.2 = (bf16[512,2048]{1,0:T(8,128)(2,1)S(1)}, bf16[512,2048]{1,0:T(8,128)(2,1)}, u32[]{:S(2)}) copy-start(bf16[512,2048]{1,0:T(8,128)(2,1)} %convolution_convert_fusion.3) | copy-start | bytes 6291460
Sparse Core Ops, SparseCore 0:
  8.9 13.2 all-gather.7
  25.0 76.7 all-gather.11
  104.5 74.1 all-gather.9
  181.3 87.3 all-gather.13
  283.3 19.4 all-reduce.4
  305.5 113.4 all-gather.15
  421.7 110.4 all-gather.17
  534.9 139.9 all-gather.19
  685.0 7.7 reduce-scatter.1
where the time goes:
time: 702 us
  waiting for transfers between devices  605 us (86%)
  matrix products  54.3 us (8%)
  other arithmetic  18.7 us (3%)
  between operations  13.3 us (2%)
    all_gather x1, waiting for transfers between devices, on_device(): whole_down = lax.all_gather(proj_down, 'fs', axis=1, tiled=True)  129 us
    all_gather x1, waiting for transfers between devices, on_device(): lax.all_gather(ffn_gate, 'fs', axis=0, tiled=True)  112 us
    all_gather x1, waiting for transfers between devices, on_device(): lax.all_gather(ffn_value, 'fs', axis=0, tiled=True)  103 us
    all_gather x1, waiting for transfers between devices, on_device(): whole_out = lax.all_gather(proj_out, 'fs', axis=1, tiled=True)  89.9 us
    all_gather x1, waiting for transfers between devices, on_device(): lax.all_gather(proj_v, 'fs', axis=0, tiled=True)  77.3 us
    all_gather x1, waiting for transfers between devices, on_device(): lax.all_gather(proj_u, 'fs', axis=0, tiled=True)  57.5 us
    dot_general x5, matrix products, matmul(): return jnp.dot(operand, matrix, preferred_element_type=jnp.float32)  52.5 us
    psum x1, waiting for transfers between devices, on_device(): lax.psum(partial_value.astype(jnp.bfloat16), 'tp').astype(jnp.float32)  15.4 us
  transfers between devices with their start and end apart: 9, of which 9 were waited for; matrix products, arithmetic and copies ran while one was open for 7% of the time, Pallas kernels for 0%

commit v1 on v0

--- a/solution.py
+++ b/solution.py
@@ -101,7 +101,9 @@
     conv_g = causal_taps(pre_gate.astype(jnp.bfloat16), conv_gate)
     conv_v = causal_taps(pre_value.astype(jnp.bfloat16), conv_value)
     hidden = (jax.nn.silu(conv_g) * conv_v).astype(jnp.bfloat16)
-    whole_down = lax.all_gather(proj_down, "fs", axis=1, tiled=True)
+    whole_down = jnp.concatenate(
+        lax.all_to_all(jnp.stack(lax.axis_size("fs") * [proj_down]), "fs", 0, 0), axis=1
+    )
     partial_two = matmul(hidden, whole_down)
     return (
         stream.astype(jnp.float32)

time: 702 us -> 706 us (level)
    all_gather x1, waiting for transfers between devices: 112 us -> 244 us  [on_device(): lax.all_gather(ffn_gate, 'fs', axis=0, tiled=True)]
    all_gather x1 -> x0, waiting for transfers between devices: 129 us -> none  [on_device(): whole_down = lax.all_gather(proj_down, 'fs', axis=1, tiled=True)]
    all_gather x1, waiting for transfers between devices: 89.9 us -> 70.6 us  [on_device(): whole_out = lax.all_gather(proj_out, 'fs', axis=1, tiled=True)]
    all_gather x1, waiting for transfers between devices: 57.5 us -> 76.4 us  [on_device(): lax.all_gather(proj_u, 'fs', axis=0, tiled=True)]
    psum x1, waiting for transfers between devices: 15.4 us -> 6.85 us  [on_device(): lax.psum(partial_value.astype(jnp.bfloat16), 'tp').astype(jnp.float32)]
  transfers between devices with their start and end apart: 9 -> 9, of which waited for: 9 -> 8; matrix products, arithmetic and copies ran while one was open for 7% -> 8% of each run, Pallas kernels for 0% -> 0%
where the time goes in v1:
time: 706 us
  waiting for transfers between devices  600 us (85%)
  matrix products  54.3 us (8%)
  other arithmetic  17.9 us (3%)
  between operations  13.6 us (2%)
  local copies, waits for them, and re-layouts  8.04 us (1%)
    all_gather x1, waiting for transfers between devices, on_device(): lax.all_gather(ffn_gate, 'fs', axis=0, tiled=True)  244 us
    all_gather x1, waiting for transfers between devices, on_device(): lax.all_gather(ffn_value, 'fs', axis=0, tiled=True)  104 us
    all_gather x1, waiting for transfers between devices, on_device(): lax.all_gather(proj_v, 'fs', axis=0, tiled=True)  77.3 us
    all_gather x1, waiting for transfers between devices, on_device(): lax.all_gather(proj_u, 'fs', axis=0, tiled=True)  76.4 us
    all_gather x1, waiting for transfers between devices, on_device(): whole_out = lax.all_gather(proj_out, 'fs', axis=1, tiled=True)  70.6 us
    dot_general x5, matrix products, matmul(): return jnp.dot(operand, matrix, preferred_element_type=jnp.float32)  52.4 us
  transfers between devices with their start and end apart: 9, of which 8 were waited for; matrix products, arithmetic and copies ran while one was open for 8% of the time, Pallas kernels for 0%

profile of v1, /device:TPU:0, one launch (start us, length us, event | category | flops | bytes accessed | tf_op | source)
XLA Modules:
  0.0 705.7 jit_solution(10779843324681756556)
XLA Ops:
  6.5 0.0 all-gather.7.cloned.1.call-start
  6.5 0.7 all-gather.7.cloned.1.call-update
  7.3 0.0 all-gather.11.cloned.1.call-start
  7.3 0.7 all-gather.11.cloned.1.call-update
  8.0 0.0 all-gather.13.cloned.1.call-start
  8.1 0.7 all-gather.13.cloned.1.call-update
  8.7 0.0 all-gather.9.cloned.1.call-start
  8.8 0.5 all-gather.9.cloned.1.call-update
  9.3 0.0 all-reduce.5.cloned.1.call-start
  9.4 2.1 all_gather.25
  11.5 0.7 convert_element_type.149
  12.2 0.7 convert_element_type.150
  12.9 0.7 convert_bitcast_fusion
  13.5 0.1 broadcast_compare_fusion
  13.6 8.6 %all-gather.7.cloned.1.call-done = bf16[512,2048]{1,0:T(8,128)(2,1)} async-done(((bf16[512,1024]{1,0:T(8,128)(2,1)}), bf16[512,2048]{1,0:T(8,128)(2,1)}) %all-gather.7.cloned.1.call-update) | async-done | bytes 2097168 | tf_op jit(solution)/shard_map/all_gather | solution.py:55
  22.2 0.0 copy-start
  22.2 2.2 fusion.3
  24.4 77.3 %all-gather.11.cloned.1.call-done = bf16[2048,1024]{1,0:T(8,128)(2,1)} async-done(((bf16[128,1024]{1,0:T(8,128)(2,1)}), bf16[2048,1024]{1,0:T(8,128)(2,1)}) %all-gather.11.cloned.1.call-update) | async-done | bytes 4194320 | tf_op jit(solution)/shard_map/all_gather | solution.py:63
  101.8 0.0 copy-done
  101.8 9.6 %fusion.107 = (f32[512]{0:T(512)S(1)}, f32[512]{0:T(512)S(1)}, f32[512,1024]{1,0:T(8,128)}) fusion(bf16[2048,1024]{1,0:T(8,128)(2,1)} %all-gather.11.cloned.1.call-done, bf16[512,2048]{1,0:T(8,128)(2,1)S(1)} %copy-done, f32[2048]{0:T(1024)S(1)} %convert_element_type.147, f32[512]{0:T(512)S(1)} %add_rsqrt_fusion.2), kind=kOutput, calls=%fused_computation.144 | convolution fusion | flops 2186804224 | bytes 8402944 | tf_op jit(solution)/shard_map/dot_general | solution.py:15
  111.4 2.6 all-reduce.2
  114.0 0.0 copy-start.4
  114.0 2.1 fusion.28
  116.1 0.3 copy.25
  116.4 0.0 copy-done.4
  116.4 1.9 bitcast_add_fusion
  118.3 3.0 copy.22
  121.2 70.6 %all-gather.13.cloned.1.call-done = bf16[1024,2048]{1,0:T(8,128)(2,1)} async-done(((bf16[1024,128]{1,0:T(8,128)(2,1)}), bf16[1024,2048]{1,0:T(8,128)(2,1)}) %all-gather.13.cloned.1.call-update) | async-done | bytes 4194320 | tf_op jit(solution)/shard_map/all_gather | solution.py:89
  191.8 76.4 %all-gather.9.cloned.1.call-done = bf16[2048,1024]{1,0:T(8,128)(2,1)} async-done(((bf16[128,1024]{1,0:T(8,128)(2,1)}), bf16[2048,1024]{1,0:T(8,128)(2,1)}) %all-gather.9.cloned.1.call-update) | async-done | bytes 4194320 | tf_op jit(solution)/shard_map/all_gather | solution.py:62
  268.3 14.4 %convolution_convert_fusion = bf16[512,2048]{1,0:T(8,128)(2,1)} fusion(bf16[1024,2048]{1,0:T(8,128)(2,1)} %all-gather.13.cloned.1.call-done, f32[64,8,8,128]{3,2,1,0:T(8,128)} %bitcast.41, bf16[2048,1024]{1,0:T(8,128)(2,1)} %all-gather.9.cloned.1.call-done, bf16[512,2048]{1,0:T(8,128)(2,1)S(1)} %copy-done, f32[2048]{0:T(1024)S(1)} %convert_element_type.147, ...), kind=kOutput, calls=%fused_computation.15 | convolution fusion | flops 4334813184 | bytes 14690304 | tf_op jit(solution)/shard_map/dot_general | solution.py:15
  282.7 0.0 copy-start.3
  282.7 0.0 all-reduce.5.cloned.1.call-update
  282.7 0.0 all-gather.15.cloned.1.call-start
  282.8 0.5 all-gather.15.cloned.1.call-update
  283.3 0.0 all-gather.17.cloned.1.call-start
  283.3 0.7 all-gather.17.cloned.1.call-update
  284.0 0.0 copy-done.3
  284.0 0.2 copy.23
  284.3 4.6 stack.2
  288.9 0.0 copy-start.7
  288.9 0.0 copy-start.5
  288.9 0.0 copy-start.6
  288.9 4.9 all-to-all-start
  293.8 0.0 reduce-scatter.2.cloned.1.call-start
  293.8 0.0 copy-done.7
  293.8 2.1 all_gather.29
  295.9 0.0 copy-done.5
  295.9 0.0 copy-done.6
  295.9 6.8 all-reduce.5.cloned.1.call-done
  302.8 3.9 fusion
  306.7 244.2 %all-gather.15.cloned.1.call-done = bf16[2048,2048]{1,0:T(8,128)(2,1)} async-done(((bf16[128,2048]{1,0:T(8,128)(2,1)}), bf16[2048,2048]{1,0:T(8,128)(2,1)}) %all-gather.15.cloned.1.call-update) | async-done | bytes 8388624 | tf_op jit(solution)/shard_map/all_gather | solution.py:96
  550.8 0.0 copy-start.1
  550.9 10.1 %convolution_convert_fusion.3 = bf16[512,2048]{1,0:T(8,128)(2,1)} fusion(bf16[2048,2048]{1,0:T(8,128)(2,1)} %all-gather.15.cloned.1.call-done, bf16[512,2048]{1,0:T(8,128)(2,1)} %get-tuple-element.10, f32[2048]{0:T(1024)S(1)} %convert_element_type.158, f32[512]{0:T(512)S(1)} %add_rsqrt_fusion), kind=kOutput, calls=%fused_computation.18 | convolution fusion | flops 4300210176 | bytes 12593152 | tf_op jit(solution)/shard_map/dot_general | solution.py:15
  560.9 104.1 %all-gather.17.cloned.1.call-done = bf16[2048,2048]{1,0:T(8,128)(2,1)} async-done(((bf16[128,2048]{1,0:T(8,128)(2,1)}), bf16[2048,2048]{1,0:T(8,128)(2,1)}) %all-gather.17.cloned.1.call-update) | async-done | bytes 8388624 | tf_op jit(solution)/shard_map/all_gather | solution.py:97
  665.0 0.0 copy-done.1
  665.0 0.0 copy-start.2
  665.0 8.4 %convolution_convert_fusion.2 = bf16[512,2048]{1,0:T(8,128)(2,1)S(1)} fusion(bf16[2048,2048]{1,0:T(8,128)(2,1)} %all-gather.17.cloned.1.call-done, bf16[512,2048]{1,0:T(8,128)(2,1)S(1)} %copy-done.1, f32[2048]{0:T(1024)S(1)} %convert_element_type.158, f32[512]{0:T(512)S(1)} %add_rsqrt_fusion), kind=kOutput, calls=%fused_computation.17 | convolution fusion | flops 4300210176 | bytes 12593152 | tf_op jit(solution)/shard_map/dot_general | solution.py:15
  673.4 0.0 copy-done.2
  673.4 4.9 multiply_convert_fusion
  678.4 0.0 all-to-all-done
  678.4 9.9 %convolution_convert_fusion.1 = bf16[512,2048]{1,0:T(8,128)(2,1)} fusion(bf16[512,2048]{1,0:T(8,128)(2,1)} %bitcast.39, bf16[2048,2048]{0,1:T(8,128)(2,1)} %bitcast.14), kind=kOutput, calls=%fused_computation.16 | convolution fusion | flops 4296015872 | bytes 12582912 | tf_op jit(solution)/shard_map/dot_general | solution.py:15
  688.3 0.0 reduce-scatter.2.cloned.1.call-update
  688.3 8.0 %reduce-scatter.2.cloned.1.call-done = bf16[512,1024]{1,0:T(8,128)(2,1)} async-done(((bf16[512,2048]{1,0:T(8,128)(2,1)}), bf16[512,1024]{1,0:T(8,128)(2,1)}) %reduce-scatter.2.cloned.1.call-update) | async-done | bytes 1048592 | tf_op jit(solution)/shard_map/reduce_scatter | solution.py:110
  696.3 2.6 add_convert_fusion
  (8 shorter events, 0.1 us)
Async XLA Ops:
  6.5 15.7 %all-gather.7.cloned.1.call-start = ((), (), s32[]{:S(2)}) async-start(), calls=%async_computation.2 | async-start | bytes 3145728 | tf_op jit(solution)/shard_map/all_gather | solution.py:55
  7.3 94.5 %all-gather.11.cloned.1.call-start = ((), (), s32[]{:S(2)}) async-start(), calls=%async_computation.4 | async-start | bytes 4456448 | tf_op jit(solution)/shard_map/all_gather | solution.py:63
  8.0 183.8 %all-gather.13.cloned.1.call-start = ((), (), s32[]{:S(2)}) async-start(), calls=%async_computation.5 | async-start | bytes 4456448 | tf_op jit(solution)/shard_map/all_gather | solution.py:89
  8.7 259.5 %all-gather.9.cloned.1.call-start = ((), (), s32[]{:S(2)}) async-start(), calls=%async_computation.3 | async-start | bytes 4456448 | tf_op jit(solution)/shard_map/all_gather | solution.py:62
  9.3 293.5 %all-reduce.5.cloned.1.call-start = ((), (), s32[]{:S(2)}) async-start(), calls=%async_computation.6 | async-start | bytes 4194304 | tf_op jit(solution)/shard_map/psum | solution.py:91
  22.2 79.6 %copy-start = (bf16[512,2048]{1,0:T(8,128)(2,1)S(1)}, bf16[512,2048]{1,0:T(8,128)(2,1)}, u32[]{:S(2)}) copy-start(bf16[512,2048]{1,0:T(8,128)(2,1)} %all-gather.7.cloned.1.call-done) | copy-start | bytes 6291460
  114.0 2.4 copy-start.4
  282.7 1.4 copy-start.3
  282.7 268.1 %all-gather.15.cloned.1.call-start = ((), (), s32[]{:S(2)}) async-start(), calls=%async_computation.7 | async-start | bytes 8912896 | tf_op jit(solution)/shard_map/all_gather | solution.py:96
  283.3 381.7 %all-gather.17.cloned.1.call-start = ((), (), s32[]{:S(2)}) async-start(), calls=%async_computation.8 | async-start | bytes 8912896 | tf_op jit(solution)/shard_map/all_gather | solution.py:97
  288.9 5.0 copy-start.7
  288.9 7.0 copy-start.5
  288.9 7.0 copy-start.6
  288.9 389.5 %all-to-all-start = ((bf16[16,2048,128]{1,2,0:T(8,128)(2,1)}), bf16[16,2048,128]{1,2,0:T(8,128)(2,1)}, u32[]{:S(2)}, u32[]{:S(2)}) async-start(bf16[16,2048,128]{1,2,0:T(8,128)(2,1)} %stack.2), calls=%async_computation | async-start | bytes 16777216 | tf_op jit(solution)/shard_map/all_to_all | solution.py:105
  293.8 402.5 %reduce-scatter.2.cloned.1.call-start = ((), (), s32[]{:S(2)}) async-start(), calls=%async_computation.9 | async-start | bytes 3145728 | tf_op jit(solution)/shard_map/reduce_scatter | solution.py:110
  550.8 114.2 %copy-start.1 = (bf16[512,2048]{1,0:T(8,128)(2,1)S(1)}, bf16[512,2048]{1,0:T(8,128)(2,1)}, u32[]{:S(2)}) copy-start(bf16[512,2048]{1,0:T(8,128)(2,1)} %get-tuple-element.10) | copy-start | bytes 6291460
  665.0 8.4 %copy-start.2 = (bf16[512,2048]{1,0:T(8,128)(2,1)S(1)}, bf16[512,2048]{1,0:T(8,128)(2,1)}, u32[]{:S(2)}) copy-start(bf16[512,2048]{1,0:T(8,128)(2,1)} %convolution_convert_fusion.3) | copy-start | bytes 6291460
Sparse Core Ops, SparseCore 0:
  8.9 13.2 all-gather.6
  25.0 76.7 all-gather.10
  104.5 87.3 all-gather.12
  194.5 73.7 all-gather.8
  282.8 19.9 all-reduce.4
  305.4 245.3 all-gather.14
  553.6 111.3 all-gather.16
  688.4 7.7 reduce-scatter.1
